TPU v7x, 32 devices: a whole 2x2x4 slice. The times are simulated.
32 devices in a mesh: sp: 8 (over z, x), tp: 4 (over y, core).
Axes of the slice: x: 2, y: 2, z: 4, core: 2. Of those that a mesh axis runs over, the one named last changes fastest.
Arguments:
- tokens: bfloat16 [2, 128, 1024], P(None, 'sp', 'tp'), may hold values from -6 to 6
- in_weight: bfloat16 [3, 1024, 2048], P(None, 'sp', 'tp'), may hold values from -0.1875 to 0.1875
- gate_weight: bfloat16 [3, 1024, 2048], P(None, 'sp', 'tp'), may hold values from -0.1875 to 0.1875
- out_weight: bfloat16 [3, 2048, 1024], P(None, 'tp', 'sp'), may hold values from -0.25 to 0.25
- recur_weight: bfloat16 [3, 2, 16, 128, 128], P(None, None, 'tp'), may hold values from -0.5 to 0.5
- input_weight: bfloat16 [3, 2, 16, 128, 128], P(None, None, 'tp'), may hold values from -0.5 to 0.5
- conv_taps: bfloat16 [3, 4, 2048], P(None, None, 'tp'), may hold values from -3 to 3
- decay_rate: float32 [3, 2, 2048], P(None, None, 'tp'), may hold values from 0.02 to 0.25
- norm_gain: float32 [3, 1024], replicated, may hold values from 0.5 to 1.5
Outputs:
- mixed_out: bfloat16 [2, 128, 1024], P(None, 'sp', 'tp')
All inputs are finite; a program needn't handle non-finite values.
Results may differ from a plain program's by a relative error of at most 0.04.
Values may be sent and summed in bfloat16 or wider, within the bound.
A program may use at most 64 MiB of HBM per device.

v0:
```python
import jax
import jax.numpy as jnp
from jax import lax
from jax.sharding import PartitionSpec as P

LAYERS = 3


epsilon = 1e-06
gate_power = 8.0


def extended(array, sides, width, wrap):
    for axis, dim in sides:
        size, length = lax.axis_size(axis), array.shape[dim]
        up = [(i, (i + 1) % size) for i in range(size if wrap else size - 1)]
        down = [(j, i) for i, j in up]
        last = lax.slice_in_dim(array, length - width, length, axis=dim)
        initial = lax.slice_in_dim(array, 0, width, axis=dim)
        before = lax.ppermute(last, axis, up)
        after = lax.ppermute(initial, axis, down)
        array = jnp.concatenate([before, array, after], axis=dim)
    return array


def carried_in(value, axis, join, neutral, backward):
    count, mine = lax.axis_size(axis), lax.axis_index(axis)
    pieces = jax.tree.map(lambda part: lax.all_gather(part, axis), value)
    if backward:
        pieces = jax.tree.map(lambda part: part[::-1], pieces)
        mine = count - 1 - mine
    subtotal = jax.tree.map(
        lambda part, zero: jnp.full_like(part, 0) + jnp.asarray(zero, part.dtype), value, neutral
    )

    def hop(position, subtotal):
        longer = join(subtotal, jax.tree.map(lambda part: part[position], pieces))
        return jax.tree.map(lambda new, old: jnp.where(position < mine, new, old), longer, subtotal)

    return lax.fori_loop(0, count - 1, hop, subtotal)


def combine(earlier, later_pair):
    first_decay, first_drive = earlier
    second_decay, second_drive = later_pair
    return (first_decay * second_decay, second_decay * first_drive + second_drive)


def body(
    tokens,
    in_weight,
    gate_weight,
    out_weight,
    recur_weight,
    input_weight,
    conv_taps,
    decay_rate,
    norm_gain,
):
    batch_size, tok_rows, _ = tokens.shape
    seq_len = tok_rows * lax.axis_size("sp")
    chan_width = in_weight.shape[2]
    in_whole, gate_whole = (
        lax.all_gather(in_weight, "sp", axis=1, tiled=True),
        lax.all_gather(gate_weight, "sp", axis=1, tiled=True),
    )
    out_whole = lax.all_gather(out_weight, "sp", axis=2, tiled=True)
    state = tokens
    for layer_index in range(LAYERS):
        gathered = lax.all_gather(state, "tp", axis=2, tiled=True)
        flat_rows = gathered.reshape(batch_size * tok_rows, -1).astype(jnp.float32)
        scale_rows = lax.rsqrt(jnp.mean(flat_rows * flat_rows, axis=-1, keepdims=True) + epsilon)
        normed = (flat_rows * scale_rows * norm_gain[layer_index]).astype(jnp.bfloat16)
        branch = jnp.dot(normed, in_whole[layer_index], preferred_element_type=jnp.float32)
        gate_branch = jnp.dot(normed, gate_whole[layer_index], preferred_element_type=jnp.float32)
        branch = branch.astype(jnp.bfloat16).reshape(batch_size, tok_rows, chan_width)
        gate_branch = gate_branch.astype(jnp.bfloat16).reshape(batch_size, tok_rows, chan_width)
        padded = extended(branch, (("sp", 1),), 2, False)
        tap_values = conv_taps[layer_index].astype(jnp.float32)
        conv_out = padded[:, 0:tok_rows].astype(jnp.float32) * tap_values[0]
        for tap_index in range(1, tap_values.shape[0]):
            conv_out = (
                conv_out
                + padded[:, tap_index : tap_index + tok_rows].astype(jnp.float32)
                * tap_values[tap_index]
            )
        conv_out = conv_out.astype(jnp.bfloat16)
        conv_float = conv_out.astype(jnp.float32)
        recur_full = recur_weight[layer_index]
        input_full = input_weight[layer_index]
        heads_local = recur_full.shape[1]
        head_dim = recur_full.shape[2]
        blocks = conv_out.reshape(batch_size, tok_rows, heads_local, head_dim)
        hidden_sum = jnp.zeros((batch_size, tok_rows, chan_width), jnp.float32)
        identity = (
            jnp.ones((batch_size, chan_width), jnp.float32),
            jnp.zeros((batch_size, chan_width), jnp.float32),
        )
        for direction in range(2):
            recur_gate = jax.nn.sigmoid(
                jnp.einsum(
                    "bthd,hde->bthe",
                    blocks,
                    recur_full[direction],
                    preferred_element_type=jnp.float32,
                )
            ).reshape(batch_size, tok_rows, chan_width)
            input_gate = jax.nn.sigmoid(
                jnp.einsum(
                    "bthd,hde->bthe",
                    blocks,
                    input_full[direction],
                    preferred_element_type=jnp.float32,
                )
            ).reshape(batch_size, tok_rows, chan_width)
            log_decay = -gate_power * recur_gate * decay_rate[layer_index, direction] / seq_len
            decay_step = jnp.exp(log_decay)
            driven = jnp.sqrt(-jnp.expm1(2.0 * log_decay)) * input_gate * conv_float
            backward = direction == 1
            cum_decay, cum_drive = lax.associative_scan(
                combine, (decay_step, driven), axis=1, reverse=backward
            )
            if backward:
                totals = (cum_decay[:, 0], cum_drive[:, 0])
                incoming = carried_in(totals, "sp", combine, identity, True)
            else:
                totals = (cum_decay[:, -1], cum_drive[:, -1])
                incoming = carried_in(totals, "sp", combine, identity, False)
            hidden_sum = hidden_sum + (cum_decay * incoming[1][:, None, :] + cum_drive)
        mixed_rows = (hidden_sum * jax.nn.silu(gate_branch.astype(jnp.float32))).astype(
            jnp.bfloat16
        )
        mixed_rows = mixed_rows.reshape(batch_size * tok_rows, chan_width)
        partial_terms = jnp.dot(
            mixed_rows, out_whole[layer_index], preferred_element_type=jnp.float32
        )
        shard_sum = lax.psum_scatter(
            partial_terms.astype(jnp.bfloat16), "tp", scatter_dimension=1, tiled=True
        ).astype(jnp.float32)
        state = shard_sum.astype(jnp.bfloat16).reshape(batch_size, tok_rows, -1)
    return state


def solution(mesh):
    in_specs = (
        P(None, "sp", "tp"),
        P(None, "sp", "tp"),
        P(None, "sp", "tp"),
        P(None, "tp", "sp"),
        P(None, None, "tp", None, None),
        P(None, None, "tp", None, None),
        P(None, None, "tp"),
        P(None, None, "tp"),
        P(),
    )
    out_specs = P(None, "sp", "tp")
    return jax.shard_map(body, mesh=mesh, in_specs=in_specs, out_specs=out_specs, check_vma=False)
```

profile of v0, /device:TPU:5, one launch (start us, length us, event | category | flops | bytes accessed | tf_op | source)
XLA Modules:
  0.0 652.1 jit_solution(7241306334868398253)
XLA Ops:
  8.8 1.4 slice_multiply_fusion.7
  10.2 1.4 fusion.178
  12.4 6.0 all_gather.54
  18.5 50.3 %all-gather.16.cloned.1.call-done = bf16[3,1024,512]{2,1,0:T(8,128)(2,1)} async-done(((bf16[3,128,512]{2,1,0:T(8,128)(2,1)}), bf16[3,1024,512]{2,1,0:T(8,128)(2,1)}) %all-gather.16.cloned.1.call-update) | async-done | bytes 3145744 | tf_op jit(solution)/shard_map/all_gather | solution.py:64
  68.8 1.5 convolution_convert_fusion.8
  70.3 1.3 collective-permute-start.1
  71.6 4.0 collective-permute-start
  75.6 54.1 %all-gather.18.cloned.1.call-done = bf16[3,1024,512]{2,1,0:T(8,128)(2,1)} async-done(((bf16[3,128,512]{2,1,0:T(8,128)(2,1)}), bf16[3,1024,512]{2,1,0:T(8,128)(2,1)}) %all-gather.18.cloned.1.call-update) | async-done | bytes 3145744 | tf_op jit(solution)/shard_map/all_gather | solution.py:65
  129.7 1.5 convolution_convert_fusion.7
  134.7 24.6 %all-gather.2 = f32[16,1,512]{2,1,0:T(1,128)S(1)} all-gather(f32[2,1,512]{2,1,0:T(1,128)S(1)} %slice_add_fusion.19), channel_id=4, replica_groups=mesh['sp'=8,'tp'=4] {'sp'}, dimensions={0}, use_global_device_ids=true | all-gather | bytes 36864 | tf_op jit(solution)/shard_map/all_gather | solution.py:28
  159.5 24.3 %all-gather.3 = f32[16,1,512]{2,1,0:T(1,128)S(1)} all-gather(f32[2,1,512]{2,1,0:T(1,128)S(1)} %slice_add_fusion.16), channel_id=5, replica_groups=mesh['sp'=8,'tp'=4] {'sp'}, dimensions={0}, use_global_device_ids=true | all-gather | bytes 36864 | tf_op jit(solution)/shard_map/all_gather | solution.py:28
  184.6 24.3 %all-gather = f32[16,1,512]{2,1,0:T(1,128)S(1)} all-gather(f32[2,1,512]{2,1,0:T(1,128)S(1)} %slice_add_fusion.23), channel_id=2, replica_groups=mesh['sp'=8,'tp'=4] {'sp'}, dimensions={0}, use_global_device_ids=true | all-gather | bytes 36864 | tf_op jit(solution)/shard_map/all_gather | solution.py:28
  209.0 24.1 %all-gather.1 = f32[16,1,512]{2,1,0:T(1,128)S(1)} all-gather(f32[2,1,512]{2,1,0:T(1,128)S(1)} %slice_add_fusion.20), channel_id=3, replica_groups=mesh['sp'=8,'tp'=4] {'sp'}, dimensions={0}, use_global_device_ids=true | all-gather | bytes 36864 | tf_op jit(solution)/shard_map/all_gather | solution.py:28
  233.9 2.1 convolution_convert_fusion.2
  236.7 43.0 %reduce-scatter.4.cloned.1.call-done = bf16[32,256]{1,0:T(8,128)(2,1)} async-done(((bf16[32,1024]{1,0:T(8,128)(2,1)}), bf16[32,256]{1,0:T(8,128)(2,1)}) %reduce-scatter.4.cloned.1.call-update) | async-done | bytes 16400 | tf_op jit(solution)/shard_map/reduce_scatter | solution.py:137
  279.7 6.3 all_gather.62
  286.2 1.5 convolution_convert_fusion.6
  287.7 1.3 collective-permute-start.3
  289.0 4.1 collective-permute-start.2
  293.1 2.1 convolution_convert_fusion.5
  297.8 1.2 fusion.37
  302.8 25.3 %all-gather.6 = f32[16,1,512]{2,1,0:T(1,128)S(1)} all-gather(f32[2,1,512]{2,1,0:T(1,128)S(1)} %slice_add_fusion.11), channel_id=8, replica_groups=mesh['sp'=8,'tp'=4] {'sp'}, dimensions={0}, use_global_device_ids=true | all-gather | bytes 36864 | tf_op jit(solution)/shard_map/all_gather | solution.py:28
  328.3 24.1 %all-gather.7 = f32[16,1,512]{2,1,0:T(1,128)S(1)} all-gather(f32[2,1,512]{2,1,0:T(1,128)S(1)} %slice_add_fusion.8), channel_id=9, replica_groups=mesh['sp'=8,'tp'=4] {'sp'}, dimensions={0}, use_global_device_ids=true | all-gather | bytes 36864 | tf_op jit(solution)/shard_map/all_gather | solution.py:28
  356.1 24.1 %all-gather.4 = f32[16,1,512]{2,1,0:T(1,128)S(1)} all-gather(f32[2,1,512]{2,1,0:T(1,128)S(1)} %slice_add_fusion.15), channel_id=6, replica_groups=mesh['sp'=8,'tp'=4] {'sp'}, dimensions={0}, use_global_device_ids=true | all-gather | bytes 36864 | tf_op jit(solution)/shard_map/all_gather | solution.py:28
  381.7 25.8 %all-gather.5 = f32[16,1,512]{2,1,0:T(1,128)} all-gather(f32[2,1,512]{2,1,0:T(1,128)S(1)} %slice_add_fusion.12), channel_id=7, replica_groups=mesh['sp'=8,'tp'=4] {'sp'}, dimensions={0}, use_global_device_ids=true | all-gather | bytes 36864 | tf_op jit(solution)/shard_map/all_gather | solution.py:28
  407.4 1.4 reduce.8
  408.9 1.4 reshape.296
  410.3 5.0 while.86
  416.1 0.9 convolution_convert_fusion.1
  417.2 43.2 %reduce-scatter.6.cloned.1.call-done = bf16[32,256]{1,0:T(8,128)(2,1)} async-done(((bf16[32,1024]{1,0:T(8,128)(2,1)}), bf16[32,256]{1,0:T(8,128)(2,1)}) %reduce-scatter.6.cloned.1.call-update) | async-done | bytes 16400 | tf_op jit(solution)/shard_map/reduce_scatter | solution.py:137
  460.4 6.3 all_gather.67
  467.6 1.5 convolution_convert_fusion.4
  469.1 1.3 collective-permute-start.5
  470.4 4.3 collective-permute-start.4
  474.7 2.1 convolution_convert_fusion.3
  477.6 1.1 fusion.17
  478.7 1.1 fusion.13
  479.8 1.1 fusion.9
  482.9 1.1 fusion.21
  487.8 25.1 %all-gather.10 = f32[16,1,512]{2,1,0:T(1,128)S(1)} all-gather(f32[2,1,512]{2,1,0:T(1,128)S(1)} %slice_add_fusion.3), channel_id=12, replica_groups=mesh['sp'=8,'tp'=4] {'sp'}, dimensions={0}, use_global_device_ids=true | all-gather | bytes 36864 | tf_op jit(solution)/shard_map/all_gather | solution.py:28
  513.1 24.1 %all-gather.11 = f32[16,1,512]{2,1,0:T(1,128)S(1)} all-gather(f32[2,1,512]{2,1,0:T(1,128)S(1)} %slice_add_fusion), channel_id=13, replica_groups=mesh['sp'=8,'tp'=4] {'sp'}, dimensions={0}, use_global_device_ids=true | all-gather | bytes 36864 | tf_op jit(solution)/shard_map/all_gather | solution.py:28
  540.9 24.1 %all-gather.8 = f32[16,1,512]{2,1,0:T(1,128)S(1)} all-gather(f32[2,1,512]{2,1,0:T(1,128)S(1)} %slice_add_fusion.7), channel_id=10, replica_groups=mesh['sp'=8,'tp'=4] {'sp'}, dimensions={0}, use_global_device_ids=true | all-gather | bytes 36864 | tf_op jit(solution)/shard_map/all_gather | solution.py:28
  566.5 25.6 %all-gather.9 = f32[16,1,512]{2,1,0:T(1,128)} all-gather(f32[2,1,512]{2,1,0:T(1,128)S(1)} %slice_add_fusion.4), channel_id=11, replica_groups=mesh['sp'=8,'tp'=4] {'sp'}, dimensions={0}, use_global_device_ids=true | all-gather | bytes 36864 | tf_op jit(solution)/shard_map/all_gather | solution.py:28
  592.1 1.4 reduce.12
  593.5 1.4 reshape.300
  594.9 5.0 while.88
  600.7 0.9 convolution_convert_fusion
  601.6 43.6 %reduce-scatter.8.cloned.1.call-done = bf16[32,256]{1,0:T(8,128)(2,1)} async-done(((bf16[32,1024]{1,0:T(8,128)(2,1)}), bf16[32,256]{1,0:T(8,128)(2,1)}) %reduce-scatter.8.cloned.1.call-update) | async-done | bytes 16400 | tf_op jit(solution)/shard_map/reduce_scatter | solution.py:137
  (488 shorter events, 44.2 us)
Async XLA Ops:
  6.5 124.8 %copy-start.3 = (bf16[3,2,4,128,128]{4,3,2,1,0:T(8,128)(2,1)S(1)}, bf16[3,2,4,128,128]{4,3,2,1,0:T(8,128)(2,1)}, u32[]{:S(2)}) copy-start(bf16[3,2,4,128,128]{4,3,2,1,0:T(8,128)(2,1)} %param.26) | copy-start | bytes 2359300
  6.5 125.1 %copy-start.4 = (bf16[3,2,4,128,128]{4,3,2,1,0:T(8,128)(2,1)S(1)}, bf16[3,2,4,128,128]{4,3,2,1,0:T(8,128)(2,1)}, u32[]{:S(2)}) copy-start(bf16[3,2,4,128,128]{4,3,2,1,0:T(8,128)(2,1)} %param.25) | copy-start | bytes 2359300
  6.5 62.3 %all-gather.16.cloned.1.call-start = ((), (), s32[]{:S(2)}) async-start(), calls=%async_computation.3 | async-start | bytes 3538944 | tf_op jit(solution)/shard_map/all_gather | solution.py:64
  7.3 122.5 %all-gather.18.cloned.1.call-start = ((), (), s32[]{:S(2)}) async-start(), calls=%async_computation.4 | async-start | bytes 3538944 | tf_op jit(solution)/shard_map/all_gather | solution.py:65
  8.0 225.9 %all-gather.20.cloned.1.call-start = ((), (), s32[]{:S(2)}) async-start(), calls=%async_computation.5 | async-start | bytes 3538944 | tf_op jit(solution)/shard_map/all_gather | solution.py:67
  8.7 270.9 %reduce-scatter.4.cloned.1.call-start = ((), (), s32[]{:S(2)}) async-start(), calls=%async_computation.6 | async-start | bytes 81920 | tf_op jit(solution)/shard_map/reduce_scatter | solution.py:137
  70.3 60.9 %collective-permute-start.1 = (bf16[2,2,512]{2,1,0:T(2,128)(2,1)S(1)}, bf16[2,2,512]{2,1,0:T(2,128)(2,1)S(1)}, u32[]{:S(2)}, u32[]{:S(2)}) collective-permute-start(bf16[2,2,512]{2,1,0:T(2,128)(2,1)S(1)} %get-tuple-element.783), channel_id=1, source_target_pairs={{4,0},{8,4},{12,8},{16,12},{20,16},{24,20},{28,24},{5,1},{9,5},{13... | collective-permute-start | bytes 12296 | tf_op jit(solution)/shard_map/ppermute | solution.py:21
  71.6 59.6 %collective-permute-start = (bf16[2,2,512]{2,1,0:T(2,128)(2,1)S(1)}, bf16[2,2,512]{2,1,0:T(2,128)(2,1)S(1)}, u32[]{:S(2)}, u32[]{:S(2)}) collective-permute-start(bf16[2,2,512]{2,1,0:T(2,128)(2,1)S(1)} %get-tuple-element.784), channel_id=1, source_target_pairs={{0,4},{4,8},{8,12},{12,16},{16,20},{20,24},{24,28},{1,5},{5,9},{9,... | collective-permute-start | bytes 12296 | tf_op jit(solution)/shard_map/ppermute | solution.py:20
  236.0 224.4 %reduce-scatter.6.cloned.1.call-start = ((), (), s32[]{:S(2)}) async-start(), calls=%async_computation.7 | async-start | bytes 81920 | tf_op jit(solution)/shard_map/reduce_scatter | solution.py:137
  287.7 7.5 %collective-permute-start.3 = (bf16[2,2,512]{2,1,0:T(2,128)(2,1)S(1)}, bf16[2,2,512]{2,1,0:T(2,128)(2,1)S(1)}, u32[]{:S(2)}, u32[]{:S(2)}) collective-permute-start(bf16[2,2,512]{2,1,0:T(2,128)(2,1)S(1)} %get-tuple-element.773), channel_id=1, source_target_pairs={{4,0},{8,4},{12,8},{16,12},{20,16},{24,20},{28,24},{5,1},{9,5},{13... | collective-permute-start | bytes 12296 | tf_op jit(solution)/shard_map/ppermute | solution.py:21
  289.0 6.2 collective-permute-start.2
  297.7 118.4 %copy-start = (bf16[3,512,1024]{2,1,0:T(8,128)(2,1)S(1)}, bf16[3,512,1024]{2,1,0:T(8,128)(2,1)}, u32[]{:S(2)}) copy-start(bf16[3,512,1024]{2,1,0:T(8,128)(2,1)} %all-gather.20.cloned.1.call-done) | copy-start | bytes 9437188
  353.1 123.8 %copy-start.2 = (f32[1,1,512]{2,1,0:T(1,128)S(1)}, f32[1,1,512]{2,1,0:T(1,128)}, u32[]{:S(2)}) copy-start(f32[1,1,512]{2,1,0:T(1,128)} %get-tuple-element.857) | copy-start | bytes 6148
  380.9 99.9 %copy-start.1 = (f32[1,1,512]{2,1,0:T(1,128)S(1)}, f32[1,1,512]{2,1,0:T(1,128)}, u32[]{:S(2)}) copy-start(f32[1,1,512]{2,1,0:T(1,128)} %get-tuple-element.841) | copy-start | bytes 6148
  417.1 228.2 %reduce-scatter.8.cloned.1.call-start = ((), (), s32[]{:S(2)}) async-start(), calls=%async_computation.8 | async-start | bytes 81920 | tf_op jit(solution)/shard_map/reduce_scatter | solution.py:137
  469.1 7.7 %collective-permute-start.5 = (bf16[2,2,512]{2,1,0:T(2,128)(2,1)S(1)}, bf16[2,2,512]{2,1,0:T(2,128)(2,1)S(1)}, u32[]{:S(2)}, u32[]{:S(2)}) collective-permute-start(bf16[2,2,512]{2,1,0:T(2,128)(2,1)S(1)} %get-tuple-element.763), channel_id=1, source_target_pairs={{4,0},{8,4},{12,8},{16,12},{20,16},{24,20},{28,24},{5,1},{9,5},{13... | collective-permute-start | bytes 12296 | tf_op jit(solution)/shard_map/ppermute | solution.py:21
  470.4 6.4 collective-permute-start.4
Sparse Core Ops, SparseCore 0:
  9.5 59.2 all-gather.15
  71.0 58.7 all-gather.17
  131.8 64.2 all-gather.19
  236.2 43.4 reduce-scatter.3
  417.2 43.1 reduce-scatter.5
  601.8 43.4 reduce-scatter.7
where the time goes:
time: 657 us; the launch traced here: 652 us
  blocking collectives  314 us (48%)
  waiting for transfers between devices  236 us (36%)
  other arithmetic  28.7 us (4%)
  matrix products  20.8 us (3%)
  local copies, waits for them, and re-layouts  19.3 us (3%)
  starting transfers between devices  16.4 us (2%)
  between operations  15.6 us (2%)
    all_gather x12, blocking collectives, carried_in(): pieces = jax.tree.map(lambda part: lax.all_gather(part, axis), value)  295 us
    reduce_scatter x3, waiting for transfers between devices, body(): lax.psum_scatter(partial_terms.astype(jnp.bfloat16), 'tp', scatter_dimens...  130 us
    all_gather x1, waiting for transfers between devices, body(): lax.all_gather(gate_weight, 'sp', axis=1, tiled=True)  54.1 us
    all_gather x1, waiting for transfers between devices, body(): lax.all_gather(in_weight, 'sp', axis=1, tiled=True)  50.3 us
    all_gather x3, blocking collectives, body(): gathered = lax.all_gather(state, 'tp', axis=2, tiled=True)  18.6 us
  transfers between devices with their start and end apart: 12, of which 5 were waited for; matrix products, arithmetic and copies ran while one was open for 2% of the time, Pallas kernels for 0%

commit v1 on v0

--- a/solution.py
+++ b/solution.py
@@ -1,6 +1,10 @@
+import functools
+
 import jax
 import jax.numpy as jnp
 from jax import lax
+from jax.experimental import pallas as pl
+from jax.experimental.pallas import tpu as pltpu
 from jax.sharding import PartitionSpec as P
 
 LAYERS = 3
@@ -141,7 +145,425 @@
     return state
 
 
+MESH = pl.DeviceIdType.MESH
+
+
+def shifted(value, distance, fill, backward):
+    rows = value.shape[0]
+    row = lax.broadcasted_iota(jnp.int32, value.shape, 0)
+    if backward:
+        moved = pltpu.roll(value, rows - distance, axis=0)
+        return jnp.where(row < rows - distance, moved, fill)
+    moved = pltpu.roll(value, distance, axis=0)
+    return jnp.where(row >= distance, moved, fill)
+
+
+def scan_rows(decay, drive, backward):
+    distance = 1
+    while distance < decay.shape[0]:
+        drive = drive + decay * shifted(drive, distance, 0.0, backward)
+        if 2 * distance < decay.shape[0]:
+            decay = decay * shifted(decay, distance, 1.0, backward)
+        distance *= 2
+    return drive
+
+
+def one_minus_exp(value):
+    grown = jnp.exp(value)
+    safe = jnp.where(grown == 1.0, 0.5, grown)
+    return jnp.where(grown == 1.0, -value, (1.0 - safe) * value / jnp.log(safe))
+
+
+def fused_kernel(
+    sizes,
+    tok_ref,
+    in_ref,
+    gate_ref,
+    out_w_ref,
+    recur_ref,
+    input_ref,
+    taps_ref,
+    rate_ref,
+    gain_ref,
+    out_ref,
+    weights,
+    out_weights,
+    states,
+    mixed,
+    terms,
+    parts,
+    arrived,
+    last,
+    final,
+    w_send,
+    w_recv,
+    wx_send,
+    wx_recv,
+    o_send,
+    o_recv,
+    tok_send,
+    tok_recv,
+    sz_send,
+    sz_recv,
+    st_send,
+    st_recv,
+    mx_send,
+    mx_recv,
+    p_send,
+    p_recv,
+    f_send,
+    f_recv,
+):
+    batch, groups, shards, head, seq_len = sizes
+    layers = in_ref.shape[0]
+    span = tok_ref.shape[1]
+    chunk = seq_len // shards
+    me, t = lax.axis_index("sp"), lax.axis_index("tp")
+    z, x = me // batch, me % batch
+    other = batch - 1 - x
+    z_at = lambda d: (z + d) % groups
+    t_at = lambda d: (t + d) % shards
+    device = lambda zz, xx, tt: (zz * batch + xx, tt)
+    lanes = lambda index: pl.ds(pl.multiple_of(index * head, head), head)
+    pending = []
+
+    def send(src, dst, send_sem, recv_sem, target):
+        copy = pltpu.make_async_remote_copy(
+            src_ref=src,
+            dst_ref=dst,
+            send_sem=send_sem,
+            recv_sem=recv_sem,
+            device_id=target,
+            device_id_type=MESH,
+        )
+        copy.start()
+        pending.append(copy)
+
+    def receive(dst, send_sem, recv_sem):
+        pltpu.make_async_remote_copy(
+            src_ref=dst,
+            dst_ref=dst,
+            send_sem=send_sem,
+            recv_sem=recv_sem,
+            device_id=(me, t),
+            device_id_type=MESH,
+        ).wait_recv()
+
+    barrier = pltpu.get_barrier_semaphore()
+
+    def greet(target):
+        pl.semaphore_signal(barrier, inc=1, device_id=target, device_id_type=MESH)
+
+    greet(device(z, other, t))
+    for d in range(1, groups):
+        greet(device(z_at(d), x, t))
+    for d in range(1, shards):
+        greet(device(z, x, t_at(d)))
+
+    @pl.when(z != t)
+    def _():
+        for xx in range(batch):
+            greet(device(t, xx, z))
+
+    for layer in range(layers):
+        weights[layer, me, :, 0:head] = in_ref[layer, :, lanes(z)]
+        weights[layer, me, :, head : 2 * head] = gate_ref[layer, :, lanes(z)]
+        out_weights[layer, :, lanes(x)] = out_w_ref[layer]
+    rows_here = pl.ds(pl.multiple_of(x * span, span), span)
+    states[0, t, z, rows_here, :] = tok_ref[x]
+
+    @pl.when(z == t)
+    def _():
+        pl.semaphore_wait(barrier, groups + shards - 1)
+
+    @pl.when(z != t)
+    def _():
+        pl.semaphore_wait(barrier, groups + shards - 1 + batch)
+
+    def send_weights(layer):
+        for d in range(1, groups):
+            for which, ref in enumerate((in_ref, gate_ref)):
+                send(
+                    ref.at[layer, :, lanes(z_at(d))],
+                    weights.at[layer, me, :, which * head : (which + 1) * head],
+                    w_send.at[layer, d, which],
+                    w_recv.at[layer, d, which],
+                    device(z_at(d), x, t),
+                )
+
+    def send_own(layer):
+        for which, ref in enumerate((in_ref, gate_ref)):
+            send(
+                ref.at[layer, :, lanes(z)],
+                weights.at[layer, me, :, which * head : (which + 1) * head],
+                wx_send.at[layer, 0, which],
+                wx_recv.at[layer, 0, which],
+                device(z, other, t),
+            )
+
+    def send_out(layer):
+        send(
+            out_w_ref.at[layer],
+            out_weights.at[layer, :, lanes(x)],
+            o_send.at[layer],
+            o_recv.at[layer],
+            device(z, other, t),
+        )
+
+    def forward_weights(layer):
+        for d in range(1, groups):
+            block = z_at(groups - d) * batch + x
+            for which in range(2):
+                view = weights.at[layer, block, :, which * head : (which + 1) * head]
+                receive(view, w_send.at[layer, d, which], w_recv.at[layer, d, which])
+                send(
+                    view,
+                    view,
+                    wx_send.at[layer, d, which],
+                    wx_recv.at[layer, d, which],
+                    device(z, other, t),
+                )
+
+    def await_weights(layer):
+        for d in range(groups):
+            block = z_at(groups - d) * batch + other
+            for which in range(2):
+                view = weights.at[layer, block, :, which * head : (which + 1) * head]
+                receive(view, wx_send.at[layer, d, which], wx_recv.at[layer, d, which])
+
+    def spread_start(level, slot):
+        here = states.at[(level, *slot(z, t))]
+        for d in range(1, groups):
+            send(here, here, sz_send.at[level, d], sz_recv.at[level, d], device(z_at(d), x, t))
+        for d in range(1, shards):
+            send(
+                here, here, st_send.at[level, 0, d], st_recv.at[level, 0, d], device(z, x, t_at(d))
+            )
+
+    def spread_forward(level, slot):
+        for e in range(1, groups):
+            view = states.at[(level, *slot(z_at(groups - e), t))]
+            receive(view, sz_send.at[level, e], sz_recv.at[level, e])
+            for d in range(1, shards):
+                send(
+                    view,
+                    view,
+                    st_send.at[level, e, d],
+                    st_recv.at[level, e, d],
+                    device(z, x, t_at(d)),
+                )
+
+    def spread_finish(level, slot):
+        for e in range(groups):
+            for d in range(1, shards):
+                view = states.at[(level, *slot(z_at(groups - e), t_at(shards - d)))]
+                receive(view, st_send.at[level, e, d], st_recv.at[level, e, d])
+
+    by_rows = lambda zz, tt: (tt, zz)
+    by_columns = lambda zz, tt: (zz, tt)
+
+    landing = states.at[0, t, z, rows_here, :]
+    send(tok_ref.at[other], landing, tok_send.at[0], tok_recv.at[0], device(z, other, t))
+    send_weights(0)
+    send_own(0)
+    rows_there = pl.ds(pl.multiple_of(other * span, span), span)
+    receive(states.at[0, t, z, rows_there, :], tok_send.at[0], tok_recv.at[0])
+    spread_start(0, by_rows)
+    send_out(0)
+    spread_forward(0, by_rows)
+    forward_weights(0)
+    if layers > 1:
+        send_weights(1)
+    spread_finish(0, by_rows)
+
+    for layer in range(layers):
+        await_weights(layer)
+        depth = states.shape[-1]
+        pieces = [
+            states[layer, a].reshape(seq_len, depth).astype(jnp.float32) for a in range(groups)
+        ]
+        squares = sum(jnp.sum(piece * piece, axis=-1, keepdims=True) for piece in pieces)
+        scale_rows = lax.rsqrt(squares / (groups * depth) + epsilon)
+        gain = gain_ref[layer : layer + 1, :]
+        both = jnp.zeros((seq_len, 2 * head), jnp.float32)
+        for a in range(groups):
+            normed = (pieces[a] * scale_rows * gain[:, a * depth : (a + 1) * depth]).astype(
+                jnp.bfloat16
+            )
+            block = weights[layer, a * batch : (a + 1) * batch].reshape(depth, 2 * head)
+            both = both + jnp.dot(normed, block, preferred_element_type=jnp.float32)
+        branch = both[:, :head].astype(jnp.bfloat16).astype(jnp.float32)
+        gate_branch = both[:, head:].astype(jnp.bfloat16).astype(jnp.float32)
+        taps = taps_ref[layer, :, lanes(z)].astype(jnp.float32)
+        count = taps.shape[0]
+        conv_out = jnp.zeros_like(branch)
+        for k in range(count):
+            offset = k - count // 2
+            moved = branch if offset == 0 else shifted(branch, abs(offset), 0.0, offset > 0)
+            conv_out = conv_out + moved * taps[k : k + 1]
+        conv_round = conv_out.astype(jnp.bfloat16)
+        conv_float = conv_round.astype(jnp.float32)
+        hidden_sum = jnp.zeros_like(branch)
+        for direction in range(2):
+            recur_gate = jax.nn.sigmoid(
+                jnp.dot(
+                    conv_round, recur_ref[layer, direction, z], preferred_element_type=jnp.float32
+                )
+            )
+            input_gate = jax.nn.sigmoid(
+                jnp.dot(
+                    conv_round, input_ref[layer, direction, z], preferred_element_type=jnp.float32
+                )
+            )
+            rate = rate_ref[layer, direction : direction + 1, lanes(z)]
+            log_decay = recur_gate * (rate * (-gate_power / seq_len))
+            decay_step = jnp.exp(log_decay)
+            driven = jnp.sqrt(one_minus_exp(2.0 * log_decay)) * input_gate * conv_float
+            hidden_sum = hidden_sum + scan_rows(decay_step, driven, direction == 1)
+        mixed[layer, z] = (hidden_sum * gate_branch * jax.nn.sigmoid(gate_branch)).astype(
+            jnp.bfloat16
+        )
+        for d in range(1, groups):
+            here = mixed.at[layer, z]
+            send(here, here, mx_send.at[layer, d], mx_recv.at[layer, d], device(z_at(d), x, t))
+        if layer + 1 < layers:
+            send_own(layer + 1)
+            send_out(layer + 1)
+            forward_weights(layer + 1)
+        receive(out_weights.at[layer, :, lanes(other)], o_send.at[layer], o_recv.at[layer])
+        total = jnp.zeros((seq_len, batch * head), jnp.float32)
+        for d in range(groups):
+            zz = z_at(groups - d)
+            if d:
+                receive(mixed.at[layer, zz], mx_send.at[layer, d], mx_recv.at[layer, d])
+            rows = pl.ds(pl.multiple_of(zz * head, head), head)
+            total = total + jnp.dot(
+                mixed[layer, zz], out_weights[layer, rows, :], preferred_element_type=jnp.float32
+            )
+        for tt in range(shards):
+            piece = total[tt * chunk : (tt + 1) * chunk]
+            terms[tt] = piece
+            parts[layer, tt] = piece.astype(jnp.bfloat16)
+        for d in range(1, shards):
+            send(
+                parts.at[layer, t_at(d)],
+                arrived.at[layer, d],
+                p_send.at[layer, d],
+                p_recv.at[layer, d],
+                device(z, x, t_at(d)),
+            )
+        summed = terms[t]
+        for d in range(1, shards):
+            receive(arrived.at[layer, d], p_send.at[layer, d], p_recv.at[layer, d])
+            summed = summed + arrived[layer, d].astype(jnp.float32)
+        summed = summed.astype(jnp.bfloat16)
+        if layer + 1 < layers:
+            states[layer + 1, z, t] = summed
+            spread_start(layer + 1, by_columns)
+            if layer + 2 < layers:
+                send_weights(layer + 2)
+            spread_forward(layer + 1, by_columns)
+            spread_finish(layer + 1, by_columns)
+        else:
+            last[...] = summed.reshape(batch, span, summed.shape[-1])
+
+    def final_copy(e):
+        return pltpu.make_async_remote_copy(
+            src_ref=last.at[x if e == 0 else other],
+            dst_ref=final.at[x],
+            send_sem=f_send.at[e],
+            recv_sem=f_recv.at[e],
+            device_id=device(t, x if e == 0 else other, z),
+            device_id_type=MESH,
+        )
+
+    @pl.when(z != t)
+    def _():
+        final_copy(0).start()
+
+    @pl.when(z == t)
+    def _():
+        final[x] = last[x]
+
+    final_copy(1).start()
+
+    @pl.when(z != t)
+    def _():
+        receive(final.at[x], f_send.at[0], f_recv.at[0])
+
+    receive(final.at[other], f_send.at[1], f_recv.at[1])
+    out_ref[...] = final[...]
+
+    for copy in pending:
+        copy.wait_send()
+
+    @pl.when(z != t)
+    def _():
+        final_copy(0).wait_send()
+
+    final_copy(1).wait_send()
+
+
+def fused(batch, groups, shards, *args):
+    tokens, in_weight, _, out_weight = args[:4]
+    layers, rows, width = in_weight.shape
+    span, features = tokens.shape[1:]
+    head = width // groups
+    seq_len = span * batch * groups
+    chunk = seq_len // shards
+    bf16, f32 = jnp.bfloat16, jnp.float32
+    dma = pltpu.SemaphoreType.DMA
+    pairs = [
+        (layers, groups, 2),
+        (layers, groups, 2),
+        (layers,),
+        (1,),
+        (layers, groups),
+        (layers, groups, shards),
+        (layers, groups),
+        (layers, shards),
+        (2,),
+    ]
+    return pl.pallas_call(
+        functools.partial(fused_kernel, (batch, groups, shards, head, seq_len)),
+        out_shape=jax.ShapeDtypeStruct(tokens.shape, tokens.dtype),
+        in_specs=[pl.BlockSpec(memory_space=pltpu.VMEM)] * len(args),
+        out_specs=pl.BlockSpec(memory_space=pltpu.VMEM),
+        scratch_shapes=[
+            pltpu.VMEM((layers, batch * groups, rows, 2 * head), bf16),
+            pltpu.VMEM((layers, width, batch * rows), bf16),
+            pltpu.VMEM((layers, groups, shards, chunk, features), bf16),
+            pltpu.VMEM((layers, groups, seq_len, head), bf16),
+            pltpu.VMEM((shards, chunk, batch * rows), f32),
+            pltpu.VMEM((layers, shards, chunk, batch * rows), bf16),
+            pltpu.VMEM((layers, shards, chunk, batch * rows), bf16),
+            pltpu.VMEM((batch, span, batch * rows), bf16),
+            pltpu.VMEM((batch, span, features), bf16),
+        ]
+        + [dma(shape) for shape in pairs for _ in range(2)],
+        compiler_params=pltpu.CompilerParams(collective_id=0, has_side_effects=True),
+    )(*args)
+
+
 def solution(mesh):
+    sp, tp = mesh.shape["sp"], mesh.shape["tp"]
+
+    def program(*args):
+        batch, span, features = args[0].shape
+        rows, width = args[1].shape[1:]
+        heads, head = args[4].shape[2:4]
+        fits = (
+            batch == 2
+            and heads * batch == sp
+            and heads == tp
+            and head == rows
+            and head % 128 == 0
+            and heads * head == width
+            and features == batch * rows
+            and span % 16 == 0
+        )
+        return fused(batch, heads, tp, *args) if fits else body(*args)
+
     in_specs = (
         P(None, "sp", "tp"),
         P(None, "sp", "tp"),
@@ -154,4 +576,6 @@
         P(),
     )
     out_specs = P(None, "sp", "tp")
-    return jax.shard_map(body, mesh=mesh, in_specs=in_specs, out_specs=out_specs, check_vma=False)
+    return jax.shard_map(
+        program, mesh=mesh, in_specs=in_specs, out_specs=out_specs, check_vma=False
+    )

time: 657 us -> 70.8 us (0.11)
  blocking collectives: 314 us -> 0 us
  waiting for transfers between devices: 236 us -> 0 us
  Pallas kernels: 0 us -> 69.3 us
  other arithmetic: 28.7 us -> 0 us
  matrix products: 20.8 us -> 0 us
  local copies, waits for them, and re-layouts: 19.3 us -> 1.32 us
  starting transfers between devices: 16.4 us -> 0 us
  between operations: 15.6 us -> 0.01 us
    all_gather x15 -> x0, blocking collectives: 314 us -> none  [the longest x12 295 us: carried_in(): pieces = jax.tree.map(lambda part: lax.all_gather(part, axis), value)]
    reduce_scatter x3 -> x0, waiting for transfers between devices: 130 us -> none  [body(): lax.psum_scatter(partial_terms.astype(jnp.bfloat16), 'tp', scatter_dimens...]
    all_gather x3 -> x0, waiting for transfers between devices: 104 us -> none  [the longest x1 54.1 us: body(): lax.all_gather(gate_weight, 'sp', axis=1, tiled=True)]
    pallas_call x0 -> x1, Pallas kernels: none -> 69.3 us  [fused(): pl.pallas_call(functools.partial(fused_kernel, (batch, groups, shards, he...]
    dot_general x21 -> x0, matrix products: 20.8 us -> none  [the longest x3 5.74 us: body(): jnp.dot(normed, gate_whole[layer_index], preferred_element_type=jnp.float32)]
    ppermute x6 -> x0, starting transfers between devices: 16.2 us -> none  [the longest x3 12.4 us: extended(): before = lax.ppermute(last, axis, up)]
    slice x144 -> x0, local copies, waits for them, and re-layouts: 11.1 us -> none  [the longest x138 9.01 us: body(): lax.associative_scan(combine, (decay_step, driven), axis=1, reverse=backw...]
    select_n x42 -> x0, other arithmetic: 10.3 us -> none  [hop(): jnp.where(position < mine, new, old)]
  transfers between devices with their start and end apart: 12 -> 0, of which waited for: 5 -> 0; matrix products, arithmetic and copies ran while one was open for 2% -> 0% of each run, Pallas kernels for 0% -> 0%
where the time goes in v1:
time: 70.8 us; the launch traced here: 70.6 us
  Pallas kernels  69.3 us (98%)
  local copies, waits for them, and re-layouts  1.32 us (2%)
    pallas_call x1, Pallas kernels, fused(): pl.pallas_call(functools.partial(fused_kernel, (batch, groups, shards, he...  69.3 us

profile of v1, /device:TPU:5, one launch (start us, length us, event | category | flops | bytes accessed | tf_op | source)
XLA Modules:
  0.0 70.6 jit_solution(16634530934860481200)
XLA Ops:
  0.0 69.3 %shard_map.91 = bf16[2,16,256]{2,1,0:T(8,128)(2,1)} custom-call(bf16[2,16,256]{2,1,0:T(8,128)(2,1)} %tok_ref.1, bf16[3,128,512]{2,1,0:T(8,128)(2,1)} %in_ref.1, bf16[3,128,512]{2,1,0:T(8,128)(2,1)} %gate_ref.1, bf16[3,512,128]{2,1,0:T(8,128)(2,1)} %out_w_ref.1, bf16[3,2,4,128,128]{4,3,2,1,0:T(8,128)(2,1)} %recur_ref.1, ...), custom_call_target="tpu_custom_call" | custom-call | tf_op jit(solution)/shard_map/pallas_call | solution.py:527
  69.3 1.3 %copy.11 = bf16[2,16,256]{2,1,0:T(8,128)(2,1)} copy(bf16[2,16,256]{2,1,0:T(8,128)(2,1)} %shard_map.91) | data formatting | bytes 32768
